TPU v7x, 256 devices: a whole 4x4x8 slice. The times are simulated.
256 devices in a mesh: sp: 64 (over z, y, core), tp: 4 (over x).
Axes of the slice: x: 4, y: 4, z: 8, core: 2. Of those that a mesh axis runs over, the one named last changes fastest.
Arguments:
- stream_in: bfloat16 [16384, 2048], P(('sp', 'tp')), may hold values from -6 to 6
- queries_one: bfloat16 [16384, 1024], P('sp', 'tp'), may hold values from -120 to 120
- queries_two: bfloat16 [16384, 1024], P('sp', 'tp'), may hold values from -120 to 120
- keys_one: bfloat16 [16384, 512], P('sp', 'tp'), may hold values from -7 to 7
- keys_two: bfloat16 [16384, 512], P('sp', 'tp'), may hold values from -7 to 7
- values: bfloat16 [16384, 1024], P('sp', 'tp'), may hold values from -6 to 6
- lambdas: float32 [8], P('tp'), may hold values from 0.3 to 0.8
- head_gain: float32 [256], replicated, may hold values from 0.1 to 1.9
- out_weight: bfloat16 [2048, 2048], P('tp'), may hold values from -0.125 to 0.125
- norm_gain: float32 [2048], replicated, may hold values from 0.1 to 1.9
- expert_ids: int32 [16384, 2], P(('sp', 'tp')), may hold values from 0 to 63, all different within a row; in each aligned block of 64 rows (0 to 63, 64 to 127, ...) at most 4 rows name the same one
- route_weight: float32 [16384, 2], P(('sp', 'tp')), may hold values from 0.1 to 1
- gate_weight: bfloat16 [64, 2048, 1024], P('sp', None, 'tp'), may hold values from -0.125 to 0.125
- up_weight: bfloat16 [64, 2048, 1024], P('sp', None, 'tp'), may hold values from -0.125 to 0.125
- down_weight: bfloat16 [64, 1024, 2048], P('sp', 'tp'), may hold values from -0.1875 to 0.1875
Outputs:
- mixed: bfloat16 [16384, 2048], P(('sp', 'tp'))
Inputs may be any that keep to these rules, and one draw needn't show every extreme that they name: `expert_ids`: each row names 2 different experts. In each aligned block of 64 rows no expert is named more than 4 times, a bound that some block reaches.
All inputs are finite; a program needn't handle non-finite values.
Results may differ from a plain program's by a relative error of at most 0.013.
Values may be sent and summed in bfloat16 or wider, within the bound.
A program may use at most 128 MiB of HBM per device.

v0:
```python
import math
import jax
import jax.numpy as jnp
from jax import lax
from jax.sharding import PartitionSpec as P

HEAD_DIM = 128
VAL_DIM = 256
EPS = 1e-06
OUT_SCALE = 0.8


def cut_along(x, dim, peers):
    before, after = (x.shape[:dim], x.shape[dim + 1 :])
    return jnp.moveaxis(x.reshape(*before, peers, -1, *after), dim, 0)


def sum_at_owner(x, axis, dim):
    peers = lax.axis_size(axis)
    tiles = lax.all_to_all(cut_along(x, dim, peers), axis, 0, 0, tiled=True)
    return jnp.sum(tiles.astype(jnp.float32), axis=0)


def update_map(carried, queries, keys, vals, allowed):
    row_max, totals, accum = carried
    scores = jnp.einsum(
        "qgrd,kgd->grqk", queries, keys, preferred_element_type=jnp.float32
    ) * HEAD_DIM ** (-0.5)
    scores = jnp.where(allowed[None, None], scores, -jnp.inf)
    new_max = jnp.maximum(row_max, jnp.max(scores, axis=-1))
    safe_max = jnp.where(new_max == -jnp.inf, 0.0, new_max)
    exp_terms = jnp.exp(scores - safe_max[..., None])
    rescale = jnp.exp(row_max - safe_max)
    totals = totals * rescale + jnp.sum(exp_terms, axis=-1)
    accum = accum * rescale[..., None] + jnp.einsum(
        "grqk,kgv->grqv", exp_terms.astype(jnp.bfloat16), vals, preferred_element_type=jnp.float32
    )
    return (new_max, totals, accum)


def fold_piece(carried, piece, q_first, q_second, query_pos, shape_info):
    kv_here, head_dim, val_dim = shape_info
    piece_rows = piece.shape[0]
    key_block = math.gcd(piece_rows, 1024)
    num_blocks = piece_rows // key_block
    last_query = jnp.max(query_pos)

    def advance(block_no, carry_now):
        first_key = block_no * key_block

        def compute(carry_in):
            rows_now = lax.dynamic_slice_in_dim(piece, block_no * key_block, key_block, 0)
            key_first = rows_now[:, : kv_here * head_dim].reshape(key_block, kv_here, head_dim)
            key_second = rows_now[:, kv_here * head_dim : 2 * kv_here * head_dim].reshape(
                key_block, kv_here, head_dim
            )
            vals = rows_now[:, 2 * kv_here * head_dim :].reshape(key_block, kv_here, val_dim)
            key_pos = first_key + lax.iota(jnp.int32, key_block)
            allowed = (key_pos[None, :] <= query_pos[:, None]) & (key_pos[None, :] >= 0)
            first_map = update_map(carry_in[0:3], q_first, key_first, vals, allowed)
            second_map = update_map(carry_in[3:6], q_second, key_second, vals, allowed)
            return first_map + second_map

        def unchanged(carry_in):
            return carry_in

        return lax.cond(first_key > last_query, unchanged, compute, carry_now)

    return lax.fori_loop(0, num_blocks, advance, carried)


def shards(
    stream_in,
    queries_one,
    queries_two,
    keys_one,
    keys_two,
    values,
    lambdas,
    head_gain,
    out_weight,
    norm_gain,
    expert_ids,
    route_weight,
    gate_weight,
    up_weight,
    down_weight,
):
    rows_q = queries_one.shape[0]
    heads_here = queries_one.shape[1] // HEAD_DIM
    kv_here = keys_one.shape[1] // HEAD_DIM
    per_kv = heads_here // kv_here
    position = lax.axis_index("sp")
    query_pos = position * rows_q + lax.iota(jnp.int32, rows_q)
    q_first = queries_one.reshape(rows_q, kv_here, per_kv, HEAD_DIM)
    q_second = queries_two.reshape(rows_q, kv_here, per_kv, HEAD_DIM)
    packed = jnp.concatenate([keys_one, keys_two, values], 1)
    shape_info = (kv_here, HEAD_DIM, VAL_DIM)
    max_init = jnp.full((kv_here, per_kv, rows_q), -jnp.inf, jnp.float32)
    sum_init = jnp.zeros((kv_here, per_kv, rows_q), jnp.float32)
    acc_init = jnp.zeros((kv_here, per_kv, rows_q, VAL_DIM), jnp.float32)
    initial = (max_init, sum_init, acc_init, max_init, sum_init, acc_init)
    final = fold_piece(
        initial,
        lax.all_gather(packed, "sp", axis=0, tiled=True),
        q_first,
        q_second,
        query_pos,
        shape_info,
    )
    mix_first = final[2] / final[1][..., None]
    mix_second = final[5] / final[4][..., None]
    difference = mix_first - lambdas.reshape(kv_here, per_kv, 1, 1) * mix_second
    mean_sq = jnp.mean(difference * difference, axis=-1, keepdims=True)
    normed_heads = (difference * lax.rsqrt(mean_sq + EPS) * head_gain * OUT_SCALE).astype(
        jnp.bfloat16
    )
    heads_out = normed_heads.transpose(2, 0, 1, 3).reshape(rows_q, heads_here * VAL_DIM)
    rows_here = stream_in.shape[0]
    picked_rows = heads_out
    attended = sum_at_owner(
        jnp.dot(picked_rows, out_weight, preferred_element_type=jnp.float32).astype(jnp.bfloat16),
        "tp",
        0,
    )
    stream = stream_in.astype(jnp.float32) + attended
    normed = (
        stream * lax.rsqrt(jnp.mean(stream * stream, axis=-1, keepdims=True) + EPS) * norm_gain
    ).astype(jnp.bfloat16)
    top_count = expert_ids.shape[1]
    experts_all = lax.axis_size("sp")
    slot_cap = 2 * top_count * rows_here // experts_all
    flat_ids = expert_ids.reshape(-1)
    one_hot = (flat_ids[:, None] == lax.iota(jnp.int32, experts_all)[None, :]).astype(jnp.int32)
    ranks = jnp.sum((jnp.cumsum(one_hot, axis=0) - 1) * one_hot, axis=1)
    slots = flat_ids * slot_cap + ranks
    selector = (slots[None, :] == lax.iota(jnp.int32, experts_all * slot_cap)[:, None]).astype(
        jnp.bfloat16
    )
    selector = jnp.sum(selector.reshape(experts_all * slot_cap, rows_here, top_count), axis=2)
    send_rows = jnp.dot(selector, normed, preferred_element_type=jnp.float32).astype(jnp.bfloat16)
    received = lax.all_to_all(send_rows, "sp", split_axis=0, concat_axis=0, tiled=True)
    all_rows = lax.all_gather(received, "tp", axis=0, tiled=True)
    picked_rows = all_rows
    gate = jnp.dot(picked_rows, gate_weight[0], preferred_element_type=jnp.float32)
    upper = jnp.dot(picked_rows, up_weight[0], preferred_element_type=jnp.float32)
    hidden = (jax.nn.silu(gate) * upper).astype(jnp.bfloat16)
    summed = lax.psum_scatter(
        jnp.dot(hidden, down_weight[0], preferred_element_type=jnp.float32).astype(jnp.bfloat16),
        "tp",
        scatter_dimension=0,
        tiled=True,
    )
    returned = lax.all_to_all(summed, "sp", split_axis=0, concat_axis=0, tiled=True)
    picked = jnp.take(returned, slots, axis=0).reshape(rows_here, top_count, -1).astype(jnp.float32)
    routed = jnp.sum(picked * route_weight[:, :, None], axis=1)
    return (stream + routed).astype(jnp.bfloat16)


def solution(mesh):
    return jax.shard_map(
        shards,
        mesh=mesh,
        in_specs=(
            P(("sp", "tp"), None),
            P("sp", "tp"),
            P("sp", "tp"),
            P("sp", "tp"),
            P("sp", "tp"),
            P("sp", "tp"),
            P("tp"),
            P(),
            P("tp", None),
            P(),
            P(("sp", "tp"), None),
            P(("sp", "tp"), None),
            P("sp", None, "tp"),
            P("sp", None, "tp"),
            P("sp", "tp", None),
        ),
        out_specs=P(("sp", "tp"), None),
        check_vma=False,
    )
```

profile of v0, /device:TPU:1, one launch (start us, length us, event | category | flops | bytes accessed | tf_op | source)
XLA Modules:
  0.0 467.8 jit_solution(7342264499680508700)
XLA Ops:
  6.5 1.8 pad_maximum_fusion
  8.4 0.0 all-gather.3.cloned.1.call-update
  8.4 0.7 add_reduce_fusion
  9.1 1.0 copy.46
  10.1 0.1 copy.48
  10.2 1.0 copy.47
  11.2 0.1 copy.49
  11.4 102.2 %all-gather.3.cloned.1.call-done = bf16[16384,512]{1,0:T(8,128)(2,1)} async-done(((bf16[256,512]{1,0:T(8,128)(2,1)}), bf16[16384,512]{1,0:T(8,128)(2,1)}) %all-gather.3.cloned.1.call-update) | async-done | bytes 16777232 | tf_op jit(solution)/shard_map/all_gather | solution.py:105
  113.7 19.9 %while.24 = (s32[]{:T(128)}, f32[1,2,256]{2,1,0:T(2,128)S(1)}, f32[1,2,256]{2,1,0:T(2,128)S(1)}, f32[1,2,256,256]{3,2,1,0:T(8,128)S(1)}, f32[1,2,256]{2,1,0:T(2,...) while((s32[]{:T(128)}, f32[1,2,256]{2,1,0:T(2,128)S(1)}, ...), condition=%wide.region_8.9_spmd.clone, body=%wide.region_1.8_spmd.clone.sunk | while | flops 813707520 | bytes 17390044 | solution.py:69
  114.4 7.3 %conditional.3 = (f32[1,2,256]{2,1,0:T(2,128)S(1)}, f32[1,2,256]{2,1,0:T(2,128)S(1)}, f32[1,2,256,256]{3,2,1,0:T(8,128)S(1)}, f32[1,2,256]{2,1,0:T(2,128)S(1)}, ...) conditional(s32[]{:T(128)} %convert_element_type.98, (s32[]{:T(128)}, s32[]{:T(128)}, s32[]{:T(128)}, ...), branch_computations={%region_2.6_spmd, %region_7.7_spmd} | conditional | flops 813707520 | bytes 17380510 | solution.py:67
  114.5 0.3 compare_and_fusion
  114.8 1.4 fusion.43
  116.3 0.3 fusion.5
  116.6 1.7 fusion.7
  118.2 1.4 fusion.42
  119.7 1.7 fusion.6
  121.4 0.3 fusion.3
  133.6 0.0 copy-start.8
  133.6 0.0 copy-start.6
  133.6 1.0 copy.51
  134.6 0.2 copy.50
  134.8 1.2 multiply_reduce_fusion.2
  136.1 0.0 copy-done.6
  136.1 0.1 multiply_convert_fusion.1
  136.2 0.0 copy-start.4
  136.2 1.7 convolution_convert_fusion.1
  137.9 4.1 all-to-all-start
  142.0 0.1 copy.52
  142.1 0.1 reshape.217
  142.3 0.1 fusion.37
  142.4 0.2 reduce_window_sum.11
  142.5 0.2 select_reduce_fusion
  142.7 0.1 reduce_sum.86
  142.9 0.1 copy.53
  143.0 0.1 fusion.36
  143.1 13.6 %all-to-all-done = bf16[4,64,2048]{2,1,0:T(8,128)(2,1)S(1)} async-done(((bf16[4,64,2048]{2,1,0:T(8,128)(2,1)}), bf16[4,64,2048]{2,1,0:T(8,128)(2,1)S(1)}, u32[]{:S(2)}, u32[]{:S(2)}) %all-to-all-start) | async-done | bytes 1048608 | tf_op jit(solution)/shard_map/all_to_all | solution.py:20
  156.7 0.2 convert_reduce_fusion
  156.9 0.2 multiply_reduce_fusion.1
  157.0 0.6 copy-done.1
  157.7 0.5 convolution_convert_fusion.2
  158.1 1.2 all_to_all.20
  159.4 142.1 %all_to_all.29 = bf16[64,4,2048]{2,1,0:T(4,128)(2,1)S(1)} all-to-all(bf16[64,4,2048]{2,1,0:T(4,128)(2,1)} %all_to_all.20), channel_id=1, replica_groups=mesh['sp'=64,'tp'=4] {'sp'}, dimensions={0} | all-to-all | bytes 2097152 | tf_op jit(solution)/shard_map/all_to_all | solution.py:142
  301.5 1.1 all_to_all.22
  302.6 0.0 all-gather.5.cloned.1.call-update
  302.6 0.0 copy-start.9
  302.7 0.2 reduce-scatter.2.cloned.1.call-start
  302.9 45.5 %all-gather.5.cloned.1.call-done = bf16[1024,2048]{1,0:T(8,128)(2,1)} async-done(((bf16[256,2048]{1,0:T(8,128)(2,1)}), bf16[1024,2048]{1,0:T(8,128)(2,1)}) %all-gather.5.cloned.1.call-update) | async-done | bytes 4194320 | tf_op jit(solution)/shard_map/all_gather | solution.py:143
  348.4 4.8 %fusion.25 = f32[1024,256]{1,0:T(8,128)} fusion(bf16[1024,2048]{1,0:T(8,128)(2,1)} %all-gather.5.cloned.1.call-done, bf16[1,2048,256]{2,1,0:T(8,128)(2,1)} %param.31), kind=kOutput, calls=%fused_computation.48 | convolution fusion | flops 1073741824 | bytes 6291456 | tf_op jit(solution)/shard_map/dot_general | solution.py:145
  353.2 9.1 %convolution_convert_fusion = bf16[1024,2048]{1,0:T(8,128)(2,1)} fusion(bf16[1024,2048]{1,0:T(8,128)(2,1)} %all-gather.5.cloned.1.call-done, bf16[1,256,2048]{2,1,0:T(8,128)(2,1)S(1)} %copy-done.9, bf16[1,2048,256]{2,1,0:T(8,128)(2,1)} %param.32, f32[1024,256]{1,0:T(8,128)} %fusion.25), kind=kOutput, calls=%fused_computation.40 | convolution fusion | flops 2151153664 | bytes 11534336 | tf_op jit(solution)/shard_map/dot_general | solution.py:149
  362.3 0.0 reduce-scatter.2.cloned.1.call-update
  362.3 0.0 copy-start.7
  362.4 50.0 %reduce-scatter.2.cloned.1.call-done = bf16[256,2048]{1,0:T(8,128)(2,1)} async-done(((bf16[1024,2048]{1,0:T(8,128)(2,1)}), bf16[256,2048]{1,0:T(8,128)(2,1)}) %reduce-scatter.2.cloned.1.call-update) | async-done | bytes 1048592 | tf_op jit(solution)/shard_map/reduce_scatter | solution.py:148
  412.4 2.3 all_to_all.23
  414.6 10.9 %all-to-all-start.2 = ((bf16[64,4,2048]{2,1,0:T(4,128)(2,1)}), bf16[64,4,2048]{2,1,0:T(4,128)(2,1)}, u32[]{:S(2)}, u32[]{:S(2)}) async-start(bf16[64,4,2048]{2,1,0:T(4,128)(2,1)} %all_to_all.23), calls=%async_computation.3 | async-start | bytes 2097152 | tf_op jit(solution)/shard_map/all_to_all | solution.py:154
  425.6 0.1 copy.55
  425.7 0.1 mul.170
  425.8 0.1 copy.56
  425.9 0.1 copy.54
  426.1 27.6 %all-to-all-done.2 = bf16[64,4,2048]{2,1,0:T(4,128)(2,1)} async-done(((bf16[64,4,2048]{2,1,0:T(4,128)(2,1)}), bf16[64,4,2048]{2,1,0:T(4,128)(2,1)}, u32[]{:S(2)}, u32[]{:S(2)}) %all-to-all-start.2) | async-done | bytes 1048608 | tf_op jit(solution)/shard_map/all_to_all | solution.py:154
  453.7 1.3 all_to_all.25
  455.0 1.7 gather_fusion
  456.7 1.4 gather.7
  458.2 2.3 multiply_reduce_fusion
  460.5 0.8 add_convert_fusion
  (128 shorter events, 1.1 us)
Async XLA Ops:
  6.5 129.7 %copy-start = (bf16[512,2048]{1,0:T(8,128)(2,1)S(1)}, bf16[512,2048]{1,0:T(8,128)(2,1)}, u32[]{:S(2)}) copy-start(bf16[512,2048]{1,0:T(8,128)(2,1)} %param.27) | copy-start | bytes 6291460
  6.5 107.1 %all-gather.3.cloned.1.call-start = ((), (), s32[]{:S(2)}) async-start(), calls=%async_computation.4 | async-start | bytes 17039360 | tf_op jit(solution)/shard_map/all_gather | solution.py:105
  133.6 1.2 copy-start.8
  133.6 2.4 copy-start.6
  136.2 5.8 %copy-start.4 = (s32[64,2]{0,1:T(2,128)S(1)}, s32[64,2]{0,1:T(2,128)}, u32[]{:S(2)}) copy-start(s32[64,2]{0,1:T(2,128)} %param.29) | copy-start | bytes 1540
  137.9 18.9 %copy-start.3 = (bf16[64,2048]{1,0:T(8,128)(2,1)S(1)}, bf16[64,2048]{1,0:T(8,128)(2,1)}, u32[]{:S(2)}) copy-start(bf16[64,2048]{1,0:T(8,128)(2,1)} %param.19) | copy-start | bytes 786436
  137.9 19.7 %copy-start.5 = (f32[2048]{0:T(1024)S(1)}, f32[2048]{0:T(1024)}, u32[]{:S(2)}) copy-start(f32[2048]{0:T(1024)} %param.28) | copy-start | bytes 24580
  137.9 18.7 %all-to-all-start = ((bf16[4,64,2048]{2,1,0:T(8,128)(2,1)}), bf16[4,64,2048]{2,1,0:T(8,128)(2,1)S(1)}, u32[]{:S(2)}, u32[]{:S(2)}) async-start(bf16[4,64,2048]{2,1,0:T(8,128)(2,1)} %bitcast.93), calls=%async_computation | async-start | bytes 2097152 | tf_op jit(solution)/shard_map/all_to_all | solution.py:20
  142.0 206.4 %all-gather.5.cloned.1.call-start = ((), (), s32[]{:S(2)}) async-start(), calls=%async_computation.5 | async-start | bytes 5242880 | tf_op jit(solution)/shard_map/all_gather | solution.py:143
  156.9 0.8 copy-start.1
  302.6 50.6 %copy-start.9 = (bf16[1,256,2048]{2,1,0:T(8,128)(2,1)S(1)}, bf16[1,256,2048]{2,1,0:T(8,128)(2,1)}, u32[]{:S(2)}) copy-start(bf16[1,256,2048]{2,1,0:T(8,128)(2,1)} %param.33) | copy-start | bytes 3145732
  302.7 109.7 %reduce-scatter.2.cloned.1.call-start = ((), (), s32[]{:S(2)}) async-start(), calls=%async_computation.6 | async-start | bytes 5242880 | tf_op jit(solution)/shard_map/reduce_scatter | solution.py:148
  362.3 63.5 %copy-start.7 = (f32[64,2]{0,1:T(2,128)S(1)}, f32[64,2]{0,1:T(2,128)}, u32[]{:S(2)}) copy-start(f32[64,2]{0,1:T(2,128)} %param.30) | copy-start | bytes 1540
  414.6 39.0 %all-to-all-start.2 = ((bf16[64,4,2048]{2,1,0:T(4,128)(2,1)}), bf16[64,4,2048]{2,1,0:T(4,128)(2,1)}, u32[]{:S(2)}, u32[]{:S(2)}) async-start(bf16[64,4,2048]{2,1,0:T(4,128)(2,1)} %all_to_all.23), calls=%async_computation.3 | async-start | bytes 2097152 | tf_op jit(solution)/shard_map/all_to_all | solution.py:154
  456.7 3.8 copy-start.2
Sparse Core Ops, SparseCore 0:
  10.1 103.4 all-gather.2
  302.8 45.6 all-gather.4
  362.5 49.8 reduce-scatter.1
where the time goes:
time: 471 us; the launch traced here: 468 us
  waiting for transfers between devices  239 us (51%)
  blocking collectives  142 us (30%)
  matrix products  22.3 us (5%)
  starting transfers between devices  15.3 us (3%)
  local copies, waits for them, and re-layouts  14.3 us (3%)
  between operations  13.4 us (3%)
  loops' own time  12.5 us (3%)
  other arithmetic  8.84 us (2%)
    all_to_all x1, blocking collectives, shards(): lax.all_to_all(send_rows, 'sp', split_axis=0, concat_axis=0, tiled=True)  142 us
    all_gather x1, waiting for transfers between devices, shards(): lax.all_gather(packed, 'sp', axis=0, tiled=True)  102 us
    reduce_scatter x1, waiting for transfers between devices, shards(): lax.psum_scatter(jnp.dot(hidden, down_weight[0], preferred_element_type=j...  50 us
    all_gather x1, waiting for transfers between devices, shards(): all_rows = lax.all_gather(received, 'tp', axis=0, tiled=True)  45.5 us
    all_to_all x1, waiting for transfers between devices, shards(): lax.all_to_all(summed, 'sp', split_axis=0, concat_axis=0, tiled=True)  27.6 us
    all_to_all x1, waiting for transfers between devices, sum_at_owner(): tiles = lax.all_to_all(cut_along(x, dim, peers), axis, 0, 0, tiled=True)  13.6 us
    another operation x1, loops' own time, fold_piece(): return lax.fori_loop(0, num_blocks, advance, carried)  11.8 us
    all_to_all x1, starting transfers between devices, shards(): lax.all_to_all(summed, 'sp', split_axis=0, concat_axis=0, tiled=True)  10.9 us
  transfers between devices with their start and end apart: 5, of which 5 were waited for; matrix products, arithmetic and copies ran while one was open for 1% of the time, Pallas kernels for 0%

commit v1 on v0

--- a/solution.py
+++ b/solution.py
@@ -100,14 +100,16 @@
     sum_init = jnp.zeros((kv_here, per_kv, rows_q), jnp.float32)
     acc_init = jnp.zeros((kv_here, per_kv, rows_q, VAL_DIM), jnp.float32)
     initial = (max_init, sum_init, acc_init, max_init, sum_init, acc_init)
-    final = fold_piece(
-        initial,
-        lax.all_gather(packed, "sp", axis=0, tiled=True),
-        q_first,
-        q_second,
-        query_pos,
-        shape_info,
+    number_things = lambda target: jnp.concatenate(
+        lax.all_to_all(
+            jnp.stack([target for _ in range(lax.axis_size("sp"))]),
+            "sp",
+            split_axis=0,
+            concat_axis=0,
+        ),
+        axis=0,
     )
+    final = fold_piece(initial, number_things(packed), q_first, q_second, query_pos, shape_info)
     mix_first = final[2] / final[1][..., None]
     mix_second = final[5] / final[4][..., None]
     difference = mix_first - lambdas.reshape(kv_here, per_kv, 1, 1) * mix_second

time: 471 us -> 814 us (1.73)
  waiting for transfers between devices: 239 us -> 498 us
  blocking collectives: 142 us -> 200 us
  starting transfers between devices: 15.3 us -> 29 us
  local copies, waits for them, and re-layouts: 14.3 us -> 23.2 us
    all_to_all x0 -> x1, waiting for transfers between devices: none -> 361 us  [shards(): lax.all_to_all(jnp.stack([target for _ in range(lax.axis_size('sp'))]), '...]
    all_gather x1 -> x0, waiting for transfers between devices: 102 us -> none  [shards(): lax.all_gather(packed, 'sp', axis=0, tiled=True)]
    all_to_all x1, blocking collectives: 142 us -> 200 us  [shards(): lax.all_to_all(send_rows, 'sp', split_axis=0, concat_axis=0, tiled=True)]
    all_to_all x0 -> x1, starting transfers between devices: none -> 13.5 us  [shards(): lax.all_to_all(jnp.stack([target for _ in range(lax.axis_size('sp'))]), '...]
  transfers between devices with their start and end apart: 5 -> 5, of which waited for: 5 -> 5; matrix products, arithmetic and copies ran while one was open for 1% -> 0% of each run, Pallas kernels for 0% -> 0%
where the time goes in v1:
time: 814 us; the launch traced here: 811 us
  waiting for transfers between devices  498 us (61%)
  blocking collectives  200 us (25%)
  starting transfers between devices  29 us (4%)
  matrix products  25.5 us (3%)
  local copies, waits for them, and re-layouts  23.2 us (3%)
  between operations  13.7 us (2%)
  other arithmetic  11 us (1%)
  loops' own time  10.1 us (1%)
    all_to_all x1, waiting for transfers between devices, shards(): lax.all_to_all(jnp.stack([target for _ in range(lax.axis_size('sp'))]), '...  361 us
    all_to_all x1, blocking collectives, shards(): lax.all_to_all(send_rows, 'sp', split_axis=0, concat_axis=0, tiled=True)  200 us
    reduce_scatter x1, waiting for transfers between devices, shards(): lax.psum_scatter(jnp.dot(hidden, down_weight[0], preferred_element_type=j...  50 us
    all_gather x1, waiting for transfers between devices, shards(): all_rows = lax.all_gather(received, 'tp', axis=0, tiled=True)  45.5 us
    all_to_all x1, waiting for transfers between devices, shards(): lax.all_to_all(summed, 'sp', split_axis=0, concat_axis=0, tiled=True)  27.6 us
  transfers between devices with their start and end apart: 5, of which 5 were waited for; matrix products, arithmetic and copies ran while one was open for 0% of the time, Pallas kernels for 0%

profile of v1, /device:TPU:1, one launch (start us, length us, event | category | flops | bytes accessed | tf_op | source)
XLA Modules:
  0.0 810.6 jit_solution(5371622345128150664)
XLA Ops:
  6.5 1.1 pad_maximum_fusion
  7.7 6.1 stack.2
  13.7 13.5 %all-to-all-start = ((bf16[64,256,512]{2,1,0:T(8,128)(2,1)}), bf16[64,256,512]{2,1,0:T(8,128)(2,1)}, u32[]{:S(2)}, u32[]{:S(2)}) async-start(bf16[64,256,512]{2,1,0:T(8,128)(2,1)} %stack.2), calls=%async_computation | async-start | bytes 33554432 | tf_op jit(solution)/shard_map/all_to_all | solution.py:104
  27.2 0.6 add_reduce_fusion
  27.8 0.1 copy.46
  27.9 0.8 copy.48
  28.7 0.1 copy.47
  28.8 0.1 copy.49
  28.9 360.8 %all-to-all-done = bf16[64,256,512]{2,1,0:T(8,128)(2,1)} async-done(((bf16[64,256,512]{2,1,0:T(8,128)(2,1)}), bf16[64,256,512]{2,1,0:T(8,128)(2,1)}, u32[]{:S(2)}, u32[]{:S(2)}) %all-to-all-start) | async-done | bytes 16777248 | tf_op jit(solution)/shard_map/all_to_all | solution.py:104
  389.8 0.6 broadcast_in_dim.41
  390.4 0.6 broadcast_in_dim.41.clone
  391.0 21.0 %while.24 = (s32[]{:T(128)}, f32[1,2,256]{2,1,0:T(2,128)S(1)}, f32[1,2,256]{2,1,0:T(2,128)}, f32[1,2,256,256]{3,2,1,0:T(8,128)S(1)}, f32[1,2,256]{2,1,0:T(2,128)...) while((s32[]{:T(128)}, f32[1,2,256]{2,1,0:T(2,128)S(1)}, ...), condition=%wide.region_8.9_spmd.clone, body=%wide.region_1.8_spmd.clone.sunk | while | flops 813707520 | bytes 26335868 | solution.py:69
  391.5 10.8 %conditional.3 = (f32[1,2,256]{2,1,0:T(2,128)S(1)}, f32[1,2,256]{2,1,0:T(2,128)}, f32[1,2,256,256]{3,2,1,0:T(8,128)S(1)}, f32[1,2,256]{2,1,0:T(2,128)S(1)}, f32[...) conditional(s32[]{:T(128)} %convert_element_type.98, (s32[]{:T(128)}, s32[]{:T(128)}, s32[]{:T(128)}, ...), branch_computations={%region_2.6_spmd, %region_7.7_spmd} | conditional | flops 813707520 | bytes 26326342 | solution.py:67
  391.6 0.3 compare_and_fusion
  391.9 2.7 fusion.43
  394.6 0.6 fusion.20
  395.3 2.4 fusion.7
  397.7 1.4 fusion.42
  399.1 1.8 fusion.6
  401.0 0.3 fusion.3
  401.3 0.3 fusion.5
  401.6 0.0 copy-done.8
  401.6 0.0 copy-done.11
  401.7 0.6 copy-done.9
  412.0 1.0 copy.50
  413.0 0.2 copy.51
  413.2 1.2 multiply_reduce_fusion.2
  414.5 0.1 multiply_convert_fusion.1
  414.6 1.7 convolution_convert_fusion.1
  416.3 4.4 all-to-all-start.1
  420.7 0.0 all-gather.2.cloned.1.call-start
  420.8 0.1 copy.52
  420.9 0.1 reshape.223
  421.0 0.1 fusion.37
  421.1 0.2 reduce_window_sum.11
  421.3 0.2 select_reduce_fusion
  421.5 0.1 reduce_sum.86
  421.6 0.1 copy.53
  421.7 0.1 fusion.36
  421.8 14.1 %all-to-all-done.1 = bf16[4,64,2048]{2,1,0:T(8,128)(2,1)} async-done(((bf16[4,64,2048]{2,1,0:T(8,128)(2,1)}), bf16[4,64,2048]{2,1,0:T(8,128)(2,1)}, u32[]{:S(2)}, u32[]{:S(2)}) %all-to-all-start.1) | async-done | bytes 1048608 | tf_op jit(solution)/shard_map/all_to_all | solution.py:20
  435.9 1.4 convert_reduce_fusion
  437.4 0.2 multiply_reduce_fusion.1
  437.5 0.6 copy-done.2
  438.1 1.5 convolution_convert_fusion.2
  439.6 1.5 all_to_all.24
  441.1 200.0 %all_to_all.34 = bf16[64,4,2048]{2,1,0:T(4,128)(2,1)} all-to-all(bf16[64,4,2048]{2,1,0:T(4,128)(2,1)S(1)} %all_to_all.24), channel_id=1, replica_groups=mesh['sp'=64,'tp'=4] {'sp'}, dimensions={0} | all-to-all | bytes 2097152 | tf_op jit(solution)/shard_map/all_to_all | solution.py:144
  641.0 2.2 all_to_all.26
  643.3 0.2 reduce-scatter.2.cloned.1.call-start
  643.5 45.5 %all-gather.2.cloned.1.call-done = bf16[1024,2048]{1,0:T(8,128)(2,1)} async-done(((bf16[256,2048]{1,0:T(8,128)(2,1)}), bf16[1024,2048]{1,0:T(8,128)(2,1)}) %all-gather.2.cloned.1.call-update) | async-done | bytes 4194320 | tf_op jit(solution)/shard_map/all_gather | solution.py:145
  689.0 4.5 fusion.25
  693.5 9.4 %convolution_convert_fusion = bf16[1024,2048]{1,0:T(8,128)(2,1)} fusion(bf16[1024,2048]{1,0:T(8,128)(2,1)} %all-gather.2.cloned.1.call-done, bf16[1,256,2048]{2,1,0:T(8,128)(2,1)} %param.33, bf16[1,2048,256]{2,1,0:T(8,128)(2,1)} %param.32, f32[1024,256]{1,0:T(8,128)} %fusion.25), kind=kOutput, calls=%fused_computation.40 | convolution fusion | flops 2151153664 | bytes 11534336 | tf_op jit(solution)/shard_map/dot_general | solution.py:151
  703.0 50.0 %reduce-scatter.2.cloned.1.call-done = bf16[256,2048]{1,0:T(8,128)(2,1)} async-done(((bf16[1024,2048]{1,0:T(8,128)(2,1)}), bf16[256,2048]{1,0:T(8,128)(2,1)}) %reduce-scatter.2.cloned.1.call-update) | async-done | bytes 1048592 | tf_op jit(solution)/shard_map/reduce_scatter | solution.py:150
  752.9 2.2 all_to_all.27
  755.2 11.0 %all-to-all-start.3 = ((bf16[64,4,2048]{2,1,0:T(4,128)(2,1)}), bf16[64,4,2048]{2,1,0:T(4,128)(2,1)}, u32[]{:S(2)}, u32[]{:S(2)}) async-start(bf16[64,4,2048]{2,1,0:T(4,128)(2,1)} %all_to_all.27), calls=%async_computation.4 | async-start | bytes 2097152 | tf_op jit(solution)/shard_map/all_to_all | solution.py:156
  766.2 0.1 copy.55
  766.3 0.1 mul.170
  766.4 0.1 copy.54
  766.5 0.1 copy.56
  766.6 27.6 %all-to-all-done.3 = bf16[64,4,2048]{2,1,0:T(4,128)(2,1)} async-done(((bf16[64,4,2048]{2,1,0:T(4,128)(2,1)}), bf16[64,4,2048]{2,1,0:T(4,128)(2,1)}, u32[]{:S(2)}, u32[]{:S(2)}) %all-to-all-start.3) | async-done | bytes 1048608 | tf_op jit(solution)/shard_map/all_to_all | solution.py:156
  794.2 1.3 all_to_all.29
  795.6 1.7 gather_fusion
  797.3 2.2 gather.7
  799.5 3.4 multiply_reduce_fusion
  803.0 0.8 add_convert_fusion
  (148 shorter events, 1.2 us)
Async XLA Ops:
  6.5 408.0 %copy-start = (bf16[512,2048]{1,0:T(8,128)(2,1)S(1)}, bf16[512,2048]{1,0:T(8,128)(2,1)}, u32[]{:S(2)}) copy-start(bf16[512,2048]{1,0:T(8,128)(2,1)} %param.27) | copy-start | bytes 6291460
  13.7 14.1 %copy-start.6 = (bf16[256,256]{1,0:T(8,128)(2,1)S(1)}, bf16[256,256]{1,0:T(8,128)(2,1)}, u32[]{:S(2)}) copy-start(bf16[256,256]{1,0:T(8,128)(2,1)} %param.20) | copy-start | bytes 393220
  13.7 14.9 %copy-start.7 = (bf16[256,256]{1,0:T(8,128)(2,1)S(1)}, bf16[256,256]{1,0:T(8,128)(2,1)}, u32[]{:S(2)}) copy-start(bf16[256,256]{1,0:T(8,128)(2,1)} %param.21) | copy-start | bytes 393220
  13.7 376.0 %all-to-all-start = ((bf16[64,256,512]{2,1,0:T(8,128)(2,1)}), bf16[64,256,512]{2,1,0:T(8,128)(2,1)}, u32[]{:S(2)}, u32[]{:S(2)}) async-start(bf16[64,256,512]{2,1,0:T(8,128)(2,1)} %stack.2), calls=%async_computation | async-start | bytes 33554432 | tf_op jit(solution)/shard_map/all_to_all | solution.py:104
  395.3 2.4 copy-start.4
  399.1 2.2 copy-start.1
  401.0 0.7 copy-start.8
  401.0 0.7 copy-start.11
  401.7 0.6 copy-start.9
  401.7 0.6 copy-start.12
  412.0 1.3 copy-start.10
  412.0 1.3 copy-start.13
  412.0 1.2 copy-start.18
  412.0 2.5 copy-start.16
  414.6 6.2 copy-start.14
  416.3 21.0 %copy-start.5 = (bf16[64,2048]{1,0:T(8,128)(2,1)S(1)}, bf16[64,2048]{1,0:T(8,128)(2,1)}, u32[]{:S(2)}) copy-start(bf16[64,2048]{1,0:T(8,128)(2,1)} %param.19) | copy-start | bytes 786436
  416.3 21.8 %copy-start.15 = (f32[2048]{0:T(1024)S(1)}, f32[2048]{0:T(1024)}, u32[]{:S(2)}) copy-start(f32[2048]{0:T(1024)} %param.28) | copy-start | bytes 24580
  416.3 19.6 %all-to-all-start.1 = ((bf16[4,64,2048]{2,1,0:T(8,128)(2,1)}), bf16[4,64,2048]{2,1,0:T(8,128)(2,1)}, u32[]{:S(2)}, u32[]{:S(2)}) async-start(bf16[4,64,2048]{2,1,0:T(8,128)(2,1)} %bitcast.28), calls=%async_computation.1 | async-start | bytes 2097152 | tf_op jit(solution)/shard_map/all_to_all | solution.py:20
  420.7 268.3 %all-gather.2.cloned.1.call-start = ((), (), s32[]{:S(2)}) async-start(), calls=%async_computation.5 | async-start | bytes 5242880 | tf_op jit(solution)/shard_map/all_gather | solution.py:145
  437.3 0.8 copy-start.2
  641.0 48.0 %copy-start.19 = (bf16[1,2048,256]{2,1,0:T(8,128)(2,1)S(1)}, bf16[1,2048,256]{2,1,0:T(8,128)(2,1)}, u32[]{:S(2)}) copy-start(bf16[1,2048,256]{2,1,0:T(8,128)(2,1)} %param.31) | copy-start | bytes 3145732
  643.3 109.7 %reduce-scatter.2.cloned.1.call-start = ((), (), s32[]{:S(2)}) async-start(), calls=%async_computation.6 | async-start | bytes 5242880 | tf_op jit(solution)/shard_map/reduce_scatter | solution.py:150
  703.0 63.6 %copy-start.17 = (f32[64,2]{0,1:T(2,128)S(1)}, f32[64,2]{0,1:T(2,128)}, u32[]{:S(2)}) copy-start(f32[64,2]{0,1:T(2,128)} %param.30) | copy-start | bytes 1540
  755.2 39.0 %all-to-all-start.3 = ((bf16[64,4,2048]{2,1,0:T(4,128)(2,1)}), bf16[64,4,2048]{2,1,0:T(4,128)(2,1)}, u32[]{:S(2)}, u32[]{:S(2)}) async-start(bf16[64,4,2048]{2,1,0:T(4,128)(2,1)} %all_to_all.27), calls=%async_computation.4 | async-start | bytes 2097152 | tf_op jit(solution)/shard_map/all_to_all | solution.py:156
  797.3 5.7 copy-start.3
Sparse Core Ops, SparseCore 0:
  643.4 45.6 all-gather.1
  703.1 49.8 reduce-scatter.1
